TPU v7x, 32 devices: a whole 2x2x4 slice. The times are simulated.
32 devices in a mesh: ep: 8 (over z, y), tp: 4 (over x, core).
Axes of the slice: x: 2, y: 2, z: 4, core: 2. Of those that a mesh axis runs over, the one named last changes fastest.
Arguments:
- mixer_in: bfloat16 [3072, 2048], P(('ep', 'tp')), may hold values from -8192 to 8192
- mixer_gain: float32 [2048], replicated, may hold values from 0.1 to 1.9
- query_weight: bfloat16 [2048, 512], P(None, 'tp'), may hold values from -4 to 4
- key_weight: bfloat16 [2048, 512], P(None, 'tp'), may hold values from -4 to 4
- value_weight: bfloat16 [2048, 512], P(None, 'tp'), may hold values from -0.125 to 0.125
- head_lambda: float32 [4], P('tp'), may hold values from 0.3 to 0.8
- head_gain: float32 [128], replicated, may hold values from 0.1 to 1.9
- out_weight: bfloat16 [512, 2048], P('tp'), may hold values from -0.25 to 0.25
- expert_in: bfloat16 [3072, 2048], P(('ep', 'tp')), may hold values from -6 to 6
- expert_gain: float32 [2048], replicated, may hold values from 0.1 to 1.9
- routes: int32 [3072, 2], P(('ep', 'tp')), may hold values from 0 to 7, all different within a row; in each aligned block of 96 rows (0 to 95, 96 to 191, ...) at most 48 rows name the same one
- route_weights: float32 [3072, 2], P(('ep', 'tp')), may hold values from 0.1 to 1
- gate_weight: bfloat16 [8, 2048, 512], P('ep'), may hold values from -0.125 to 0.125
- up_weight: bfloat16 [8, 2048, 512], P('ep'), may hold values from -0.125 to 0.125
- down_weight: bfloat16 [8, 512, 2048], P('ep'), may hold values from -0.25 to 0.25
- shared_gate: bfloat16 [2048, 512], P(None, 'tp'), may hold values from -0.125 to 0.125
- shared_up: bfloat16 [2048, 512], P(None, 'tp'), may hold values from -0.125 to 0.125
- shared_down: bfloat16 [512, 2048], P('tp'), may hold values from -0.25 to 0.25
Outputs:
- mixed_out: bfloat16 [3072, 2048], P(('ep', 'tp'))
- expert_out: bfloat16 [3072, 2048], P(('ep', 'tp'))
Inputs may be any that keep to these rules, and one draw needn't show every extreme that they name: `routes`: each row names 2 different experts. Among the 96 rows of one device no expert is named more than 48 times, and in every draw some device's rows name some expert exactly 48 times.
All inputs are finite; a program needn't handle non-finite values.
Results may differ from a plain program's by a relative error of at most 0.013.
The roundings to bfloat16 on the way count: a program that leaves them out, or rounds other values in their place, can miss the bound.
Values may be sent and summed in bfloat16 or wider, within the bound.
A program may use at most 128 MiB of HBM per device.

v0:
```python
import functools
import math

import jax
import jax.numpy as jnp
from jax import lax
from jax.experimental import pallas as pl
from jax.experimental.pallas import tpu as pltpu
from jax.sharding import PartitionSpec as P

MESH = pl.DeviceIdType.MESH

EPS = 1e-06
ROUTED_SCALE = 2.5


def rms_rows(matrix, scales):
    values_in = matrix.astype(jnp.float32)
    inverse = lax.rsqrt(jnp.mean(values_in * values_in, axis=-1, keepdims=True) + EPS)
    return values_in * inverse * scales


def on_device_plain(
    mixer_in,
    mixer_gain,
    query_weight,
    key_weight,
    value_weight,
    head_lambda,
    head_gain,
    out_weight,
    expert_in,
    expert_gain,
    routes,
    route_weights,
    gate_weight,
    up_weight,
    down_weight,
    shared_gate,
    shared_up,
    shared_down,
):
    model_width = mixer_in.shape[1]
    heads_dev = head_lambda.shape[0]
    value_dim = head_gain.shape[0]
    query_cols = query_weight.shape[1]
    half_dim = query_cols // (2 * heads_dev)
    normed_mixer = rms_rows(mixer_in, mixer_gain).astype(jnp.bfloat16)
    normed_expert = rms_rows(expert_in, expert_gain).astype(jnp.bfloat16)
    joined_weight = jnp.concatenate([query_weight, key_weight, value_weight], axis=1)
    projected = jnp.dot(
        lax.all_gather(normed_mixer, "tp", axis=0, tiled=True),
        joined_weight,
        preferred_element_type=jnp.float32,
    ).astype(jnp.bfloat16)
    block_rows = lax.all_gather(normed_expert, "tp", axis=0, tiled=True)
    gate_part = jnp.dot(block_rows, shared_gate, preferred_element_type=jnp.float32)
    up_part = jnp.dot(block_rows, shared_up, preferred_element_type=jnp.float32)
    shared_hidden = (jax.nn.silu(gate_part) * up_part).astype(jnp.bfloat16)
    gathered_rows = projected.shape[0]
    queries = projected[:, :query_cols].reshape(gathered_rows, heads_dev, 2, half_dim)
    key_rows = projected[:, query_cols : 2 * query_cols]
    value_rows = projected[:, 2 * query_cols :]
    scale_factor = half_dim ** (-0.5)

    def attend_block(running, key_block, value_block):
        top_now, total_now, acc_now = running
        span = key_block.shape[0]
        key_heads = key_block.reshape(span, heads_dev, 2, half_dim)
        value_heads = value_block.reshape(span, heads_dev, value_dim)
        scores = (
            jnp.einsum("qhcd,khcd->hcqk", queries, key_heads, preferred_element_type=jnp.float32)
            * scale_factor
        )
        top_next = jnp.maximum(top_now, jnp.max(scores, axis=-1))
        exponent = jnp.exp(scores - top_next[..., None])
        rescale = jnp.exp(top_now - top_next)
        total_next = total_now * rescale + jnp.sum(exponent, axis=-1)
        product = jnp.einsum(
            "hcqk,khe->hcqe",
            exponent.astype(jnp.bfloat16),
            value_heads,
            preferred_element_type=jnp.float32,
        )
        return (top_next, total_next, acc_now * rescale[..., None] + product)

    start_state = (
        jnp.full((heads_dev, 2, gathered_rows), -1e30, jnp.float32),
        jnp.zeros((heads_dev, 2, gathered_rows), jnp.float32),
        jnp.zeros((heads_dev, 2, gathered_rows, value_dim), jnp.float32),
    )
    key_piece = lax.all_gather(key_rows, "ep", axis=0, tiled=True)
    value_piece = lax.all_gather(value_rows, "ep", axis=0, tiled=True)
    span = key_piece.shape[0]
    block_len = math.gcd(span, 4 * gathered_rows)
    steps_count = span // block_len
    key_blocks = key_piece.reshape(steps_count, block_len, key_piece.shape[1])
    value_blocks = value_piece.reshape(steps_count, block_len, value_piece.shape[1])

    def step_once(state, blocks):
        return (attend_block(state, blocks[0], blocks[1]), None)

    result, unused = lax.scan(step_once, start_state, (key_blocks, value_blocks))
    top_all, total_all, acc_all = result
    read_out = acc_all / total_all[..., None]
    lambda_col = head_lambda[:, None, None]
    difference = read_out[:, 0] - lambda_col * read_out[:, 1]
    head_out = rms_rows(difference, head_gain) * (1.0 - lambda_col)
    attended = (
        jnp.transpose(head_out, (1, 0, 2))
        .reshape(gathered_rows, heads_dev * value_dim)
        .astype(jnp.bfloat16)
    )
    token_count = routes.shape[0]
    top_count = routes.shape[1]
    ep_count = lax.axis_size("ep")
    local_experts = gate_weight.shape[0]
    expert_count = ep_count * local_experts
    capacity = 2 * token_count * top_count // expert_count
    flat_routes = routes.reshape(-1)
    onehot = (flat_routes[:, None] == jnp.arange(expert_count, dtype=jnp.int32)[None, :]).astype(
        jnp.int32
    )
    earlier = jnp.cumsum(onehot, axis=0) - onehot
    slot_rank = jnp.sum(earlier * onehot, axis=1)
    slot_index = flat_routes * capacity + slot_rank
    owners = jnp.arange(token_count * top_count, dtype=jnp.int32) // top_count
    source = jnp.full((expert_count * capacity,), token_count, jnp.int32).at[slot_index].set(owners)
    padded = jnp.concatenate([normed_expert, jnp.zeros((1, model_width), jnp.bfloat16)], axis=0)
    outgoing = padded[source].reshape(ep_count, local_experts, capacity, model_width)
    arrived = lax.all_to_all(outgoing, "ep", split_axis=0, concat_axis=0, tiled=True)
    gate_part = jnp.einsum(
        "sxcd,xdf->sxcf", arrived, gate_weight, preferred_element_type=jnp.float32
    )
    up_part = jnp.einsum("sxcd,xdf->sxcf", arrived, up_weight, preferred_element_type=jnp.float32)
    hidden = (jax.nn.silu(gate_part) * up_part).astype(jnp.bfloat16)
    result = jnp.einsum(
        "sxcf,xfd->sxcd", hidden, down_weight, preferred_element_type=jnp.float32
    ).astype(jnp.bfloat16)
    returned = lax.all_to_all(result, "ep", split_axis=0, concat_axis=0, tiled=True)
    picked = returned.reshape(expert_count * capacity, model_width)[slot_index]
    picked = picked.reshape(token_count, top_count, model_width)
    shares = ROUTED_SCALE * route_weights / jnp.sum(route_weights, axis=1, keepdims=True)
    routed = jnp.sum(shares[:, :, None] * picked.astype(jnp.float32), axis=1)
    rows_here = attended
    mixer_sum = lax.psum_scatter(
        jnp.dot(rows_here, out_weight, preferred_element_type=jnp.float32).astype(jnp.bfloat16),
        "tp",
        scatter_dimension=0,
        tiled=True,
    )
    rows_here = shared_hidden
    shared_sum = lax.psum_scatter(
        jnp.dot(rows_here, shared_down, preferred_element_type=jnp.float32).astype(jnp.bfloat16),
        "tp",
        scatter_dimension=0,
        tiled=True,
    ).astype(jnp.float32)
    expert_out = (routed + shared_sum).astype(jnp.bfloat16)
    return (mixer_sum, expert_out)


def fused_kernel(
    n_ep,
    cap,
    mixer_in,
    mixer_gain,
    wq_hbm,
    wk_hbm,
    wv_hbm,
    head_lambda,
    head_gain,
    wo_hbm,
    expert_in,
    expert_gain,
    routes_t,
    weights_t,
    gate_hbm,
    up_hbm,
    down_hbm,
    sgate_hbm,
    sup_hbm,
    sdown_hbm,
    mixed_out,
    expert_out,
    w_qkv,
    w_gate,
    w_up,
    w_down,
    w_sh,
    g_mix,
    g_exp,
    g_wo,
    g_wsd,
    outgoing,
    arrived,
    result,
    returned,
    kv_all,
    q_two,
    att_mine,
    att_all,
    hid_mine,
    hid_all,
    top_ref,
    total_ref,
    acc_ref,
    load_sem,
    tp_send,
    tp_recv,
    small_send,
    small_recv,
    ep_send,
    ep_recv,
    line_send,
    line_recv,
    twin_send,
    twin_recv,
    z_rows,
    ranks,
    slots_send,
    slots_recv,
):
    me = lax.axis_index("ep")
    tp = lax.axis_index("tp")
    near = tp + 1 - 2 * lax.rem(tp, 2)
    far = lax.rem(tp + 2, 4)
    cross = lax.rem(near + 2, 4)
    n_pair = n_ep // 2
    tokens, width = mixer_in.shape
    vdim = head_gain.shape[1]
    qcols = wq_hbm.shape[1]
    shid = sgate_hbm.shape[1]
    half = qcols // 2
    rows = 4 * tokens

    def peer_at(i):
        pair, low = me // 2, lax.rem(me, 2)
        return lax.rem(pair + i // 2, n_pair) * 2 + lax.rem(low + lax.rem(i, 2), 2)

    line, low = me // 2, lax.rem(me, 2)
    twin = 2 * line + 1 - low

    barrier = pltpu.get_barrier_semaphore()
    for other in (near, far, cross):
        pl.semaphore_signal(barrier, inc=1, device_id=(me, other), device_id_type=MESH)
    for i in range(1, n_ep):
        pl.semaphore_signal(barrier, inc=1, device_id=(peer_at(i), tp), device_id_type=MESH)

    pairs = (
        (wq_hbm, w_qkv.at[:, 0:qcols]),
        (wk_hbm, w_qkv.at[:, qcols : 2 * qcols]),
        (wv_hbm, w_qkv.at[:, 2 * qcols : 2 * qcols + vdim]),
        (sdown_hbm, g_wsd.at[tp]),
        (wo_hbm, g_wo.at[tp]),
        (sgate_hbm, w_sh.at[:, 0:shid]),
        (sup_hbm, w_sh.at[:, shid : 2 * shid]),
        (gate_hbm.at[0], w_gate),
        (up_hbm.at[0], w_up),
        (down_hbm.at[0], w_down),
    )
    loads = []
    for number, (origin, target) in enumerate(pairs):
        load = pltpu.make_async_copy(origin, target, load_sem.at[number])
        load.start()
        loads.append(load)

    def tp_copy(buf, slot, other, number):
        return pltpu.make_async_remote_copy(
            src_ref=buf.at[slot],
            dst_ref=buf.at[slot],
            send_sem=tp_send.at[number],
            recv_sem=tp_recv.at[number],
            device_id=(me, other),
            device_id_type=MESH,
        )

    def gather_start(buf, number):
        to_far = tp_copy(buf, tp, far, 3 * number)
        to_near = tp_copy(buf, tp, near, 3 * number + 1)
        to_far.start()
        to_near.start()
        return to_far, to_near

    def relay_start(buf, number, copies):
        copies[0].wait_recv()
        relay = tp_copy(buf, far, near, 3 * number + 2)
        relay.start()
        return relay

    def ep_copy(origin, target, i, number):
        return pltpu.make_async_remote_copy(
            src_ref=origin,
            dst_ref=target,
            send_sem=ep_send.at[number, i],
            recv_sem=ep_recv.at[number, i],
            device_id=(peer_at(i), tp),
            device_id_type=MESH,
        )

    def line_copy(buf, hop, way, row):
        place = line - (hop - 1) * (1 - 2 * way)
        block = 2 * place + low if row == 0 else place
        goal = lax.rem(line + (1 - 2 * way) + n_pair, n_pair)
        return pltpu.make_async_remote_copy(
            src_ref=buf.at[block],
            dst_ref=buf.at[block],
            send_sem=line_send.at[row + way, hop],
            recv_sem=line_recv.at[row + way, hop],
            device_id=(2 * goal + low, tp),
            device_id_type=MESH,
        )

    def line_wait(block, hop, way, row):
        pltpu.make_async_remote_copy(
            src_ref=block,
            dst_ref=block,
            send_sem=line_send.at[row + way, hop],
            recv_sem=line_recv.at[row + way, hop],
            device_id=(twin, tp),
            device_id_type=MESH,
        ).wait_recv()

    def sends(hop, way):
        if way == 0:
            return jnp.logical_and(line + 1 < n_pair, line - (hop - 1) >= 0)
        return jnp.logical_and(line - 1 >= 0, line + (hop - 1) < n_pair)

    def arrives(hop, way):
        return line - hop >= 0 if way == 0 else line + hop < n_pair

    g_mix[tp] = rms_rows(mixer_in[...], mixer_gain[...]).astype(jnp.bfloat16)
    pl.semaphore_wait(barrier, n_ep + 2)
    mix_copies = gather_start(g_mix, 0)
    normed = rms_rows(expert_in[...], expert_gain[...]).astype(jnp.bfloat16)
    g_exp[tp] = normed
    z_rows[line] = normed
    for way in range(2):

        @pl.when(sends(1, way))
        def _():
            line_copy(z_rows, 1, way, 2).start()

    exp_copies = gather_start(g_exp, 1)

    expert_row = lax.broadcasted_iota(jnp.int32, (n_ep, tokens), 0)
    first, second = routes_t[0:1, :] == expert_row, routes_t[1:2, :] == expert_row
    named = jnp.logical_or(first, second)
    before = (
        lax.broadcasted_iota(jnp.int32, (tokens, tokens), 0)
        < lax.broadcasted_iota(jnp.int32, (tokens, tokens), 1)
    )
    rank = jnp.dot(
        jnp.where(named, 1.0, 0.0).astype(jnp.bfloat16),
        jnp.where(before, 1.0, 0.0).astype(jnp.bfloat16),
        preferred_element_type=jnp.float32,
    )
    rank = jnp.where(named, rank, -1.0)
    scale = ROUTED_SCALE / (weights_t[0:1, :] + weights_t[1:2, :])
    share = jnp.where(first, weights_t[0:1, :] * scale, 0.0)
    share = share + jnp.where(second, weights_t[1:2, :] * scale, 0.0)
    slot = lax.broadcasted_iota(jnp.int32, (cap, tokens), 0).astype(jnp.float32)
    chosen = [rank[e : e + 1, :] == slot for e in range(n_ep)]
    combine = jnp.concatenate(
        [jnp.where(c, share[e : e + 1, :], 0.0) for e, c in enumerate(chosen)], axis=0
    )
    ranks[line] = rank

    def rank_copy(hop):
        return ep_copy(ranks.at[line], ranks.at[line], 2 * hop, 0)

    for hop in range(1, n_pair):
        rank_copy(hop).start()

    def slots_copy(place):
        return pltpu.make_async_remote_copy(
            src_ref=outgoing.at[place],
            dst_ref=arrived.at[2 * place + low],
            send_sem=slots_send.at[place],
            recv_sem=slots_recv.at[place],
            device_id=(twin, tp),
            device_id_type=MESH,
        )

    def split_rows(place):
        wanted = [ranks[place, pl.ds(e, 1), :] == slot for e in (twin, me)]
        picks = jnp.concatenate([jnp.where(c, 1.0, 0.0) for c in wanted], axis=0)
        moved = jnp.dot(
            picks.astype(jnp.bfloat16), z_rows[place], preferred_element_type=jnp.float32
        ).astype(jnp.bfloat16)
        outgoing[place] = moved[:cap]
        slots_copy(place).start()
        arrived[2 * place + low] = moved[cap:]

    def rows_forward(hop):
        for way in range(2):

            @pl.when(arrives(hop, way))
            def _():
                line_wait(z_rows.at[line - hop * (1 - 2 * way)], hop, way, 2)

            if hop + 1 < n_pair:

                @pl.when(sends(hop + 1, way))
                def _():
                    line_copy(z_rows, hop + 1, way, 2).start()

        for way in range(2):

            @pl.when(arrives(hop, way))
            def _():
                rank_copy(hop if way == 0 else n_pair - hop).wait_recv()
                split_rows(line - hop * (1 - 2 * way))

    split_rows(line)
    loads[3].wait()
    wsd_copies = gather_start(g_wsd, 2)
    loads[4].wait()
    wo_copies = gather_start(g_wo, 3)

    for number in range(3):
        loads[number].wait()

    def project(chip):
        block = g_mix[pl.ds(2 * chip, 2)].reshape(2 * tokens, width)
        out = jnp.dot(block, w_qkv[...], preferred_element_type=jnp.float32).astype(jnp.bfloat16)
        place = pl.ds(pl.multiple_of(2 * chip * tokens, 2 * tokens), 2 * tokens)
        kv_all[me, place, :] = out[:, qcols:]
        queries = out[:, :qcols].astype(jnp.float32) * (half ** (-0.5))
        lane = lax.broadcasted_iota(jnp.int32, queries.shape, 1)
        q_two[0, place, :] = jnp.where(lane < half, queries, 0.0).astype(jnp.bfloat16)
        q_two[1, place, :] = jnp.where(lane < half, 0.0, queries).astype(jnp.bfloat16)

    mix_copies[1].wait_recv()
    project(tp // 2)
    mix_relay = relay_start(g_mix, 0, mix_copies)
    if n_pair > 1:
        rows_forward(1)
    mix_relay.wait_recv()
    project(far // 2)

    def twin_copy(place):
        return pltpu.make_async_remote_copy(
            src_ref=kv_all.at[2 * place + low],
            dst_ref=kv_all.at[2 * place + low],
            send_sem=twin_send.at[place],
            recv_sem=twin_recv.at[place],
            device_id=(twin, tp),
            device_id_type=MESH,
        )

    def kv_forward(hop):
        for way in range(2):
            if hop > 0:

                @pl.when(arrives(hop, way))
                def _():
                    place = line - hop * (1 - 2 * way)
                    line_wait(kv_all.at[2 * place + low], hop, way, 0)

            if hop + 1 < n_pair:

                @pl.when(sends(hop + 1, way))
                def _():
                    line_copy(kv_all, hop + 1, way, 0).start()

            if hop > 0:

                @pl.when(arrives(hop, way))
                def _():
                    twin_copy(line - hop * (1 - 2 * way)).start()

        if hop == 0:
            twin_copy(line).start()

    kv_forward(0)

    exp_relay = relay_start(g_exp, 1, exp_copies)
    exp_copies[1].wait_recv()
    loads[5].wait()
    loads[6].wait()
    exp_relay.wait_recv()
    both = jnp.dot(
        g_exp[...].reshape(rows, width), w_sh[...], preferred_element_type=jnp.float32
    )
    hid_mine[...] = (
        (silu(both[:, :shid]) * both[:, shid:]).astype(jnp.bfloat16).reshape(4, tokens, shid)
    )

    def spread(mine, everyone, base):
        copies = []
        for k, other in enumerate((near, far, cross)):
            copy = pltpu.make_async_remote_copy(
                src_ref=mine.at[other],
                dst_ref=everyone.at[tp],
                send_sem=small_send.at[base + k],
                recv_sem=small_recv.at[base + k],
                device_id=(me, other),
                device_id_type=MESH,
            )
            copy.start()
            copies.append(copy)
        everyone[tp] = mine[tp]
        return copies

    hid_copies = spread(hid_mine, hid_all, 0)

    def back_copy(i):
        return ep_copy(result.at[peer_at(i)], returned.at[me], i, 1)

    def experts(place):
        slots_copy(place).wait_recv()
        both_cols = pl.ds(2 * place, 2)
        taken = arrived[both_cols].reshape(2 * cap, width)
        gate_part = jnp.dot(taken, w_gate[...], preferred_element_type=jnp.float32)
        up_part = jnp.dot(taken, w_up[...], preferred_element_type=jnp.float32)
        hidden = (silu(gate_part) * up_part).astype(jnp.bfloat16)
        result[both_cols] = (
            jnp.dot(hidden, w_down[...], preferred_element_type=jnp.float32)
            .astype(jnp.bfloat16)
            .reshape(2, cap, width)
        )

    def experts_at(hop):
        def one_way(way, carry):
            place = line - hop * (1 - 2 * way)

            @pl.when(jnp.logical_and(place >= 0, place < n_pair))
            def _():
                experts(place)
                number = 2 * lax.rem(place - line + n_pair, n_pair)
                back_copy(number).start()
                back_copy(number + 1).start()

            return carry

        lax.fori_loop(0, 2, one_way, 0)

    for number in range(7, 10):
        loads[number].wait()
    experts(line)
    back_copy(1).start()
    returned[me] = result[me]
    for hop in range(1, n_pair):
        kv_forward(hop)
        if hop + 1 < n_pair:
            rows_forward(hop + 1)
        experts_at(hop)
    wsd_relay = relay_start(g_wsd, 2, wsd_copies)

    top_ref[...] = jnp.full_like(top_ref, -1e30)
    total_ref[...] = jnp.zeros_like(total_ref)
    acc_ref[...] = jnp.zeros_like(acc_ref)
    chunk = rows // 3

    def attend(i, carry):
        hop, way, other = i // 4, lax.rem(i // 2, 2), lax.rem(i, 2)
        place = line - hop * (1 - 2 * way)
        inside = jnp.logical_and(place >= 0, place < n_pair)
        fresh = jnp.logical_or(hop > 0, way == 0)

        @pl.when(jnp.logical_and(inside, fresh))
        def _():
            @pl.when(other == 1)
            def _():
                twin_copy(place).wait_recv()

            origin = 2 * place + lax.rem(low + other, 2)
            keys = kv_all[origin, :, 0:qcols]
            values = kv_all[origin, :, qcols : qcols + vdim]
            for c in range(2):
                for r in range(3):
                    part = slice(r * chunk, (r + 1) * chunk)
                    scores = lax.dot_general(
                        q_two[c, part, :],
                        keys,
                        (((1,), (1,)), ((), ())),
                        preferred_element_type=jnp.float32,
                    )
                    top_now = top_ref[c, part, :]
                    top_next = jnp.maximum(top_now, jnp.max(scores, axis=1, keepdims=True))
                    exponent = jnp.exp(scores - top_next)
                    rescale = jnp.exp(top_now - top_next)
                    top_ref[c, part, :] = top_next
                    total_ref[c, part, :] = total_ref[c, part, :] * rescale + jnp.sum(
                        exponent, axis=1, keepdims=True
                    )
                    acc_ref[c, part, :] = acc_ref[c, part, :] * rescale + jnp.dot(
                        exponent.astype(jnp.bfloat16), values, preferred_element_type=jnp.float32
                    )

        return carry

    split = min(2, n_pair)
    lax.fori_loop(0, 4 * split, attend, 0)
    lax.fori_loop(4 * split, 4 * n_pair, attend, 0)
    lam = head_lambda[0]
    difference = acc_ref[0] / total_ref[0] - lam * (acc_ref[1] / total_ref[1])
    att_mine[...] = (
        (rms_rows(difference, head_gain[...]) * (1.0 - lam))
        .astype(jnp.bfloat16)
        .reshape(4, tokens, vdim)
    )
    att_copies = spread(att_mine, att_all, 3)

    wo_relay = relay_start(g_wo, 3, wo_copies)
    wsd_copies[1].wait_recv()
    wsd_relay.wait_recv()
    for copy in hid_copies:
        copy.wait_recv()

    def grouped(rows_all, weight_all):
        total = None
        for g in range(4):
            piece = (
                jnp.dot(rows_all[g], weight_all[g], preferred_element_type=jnp.float32)
                .astype(jnp.bfloat16)
                .astype(jnp.float32)
            )
            total = piece if total is None else total + piece
        return total

    shared_sum = grouped(hid_all, g_wsd)
    wo_copies[1].wait_recv()
    wo_relay.wait_recv()
    for copy in att_copies:
        copy.wait_recv()
    mixed_out[...] = grouped(att_all, g_wo).astype(jnp.bfloat16)

    high = combine.astype(jnp.bfloat16)
    rest = combine - high.astype(jnp.float32)
    middle = rest.astype(jnp.bfloat16)
    lowest = (rest - middle.astype(jnp.float32)).astype(jnp.bfloat16)
    for i in range(1, n_ep):
        back_copy(i).wait_recv()
    answers = returned[...].reshape(n_ep * cap, width)
    routed = shared_sum
    for piece in (high, middle, lowest):
        routed = routed + lax.dot_general(
            piece, answers, (((0,), (0,)), ((), ())), preferred_element_type=jnp.float32
        )
    expert_out[...] = routed.astype(jnp.bfloat16)

    for copies in (mix_copies, exp_copies, wsd_copies, wo_copies):
        for copy in copies:
            copy.wait_send()
    for copy in (mix_relay, exp_relay, wsd_relay, wo_relay):
        copy.wait_send()
    for place in range(n_pair):
        twin_copy(place).wait_send()
    for hop in range(1, n_pair):
        for way in range(2):

            @pl.when(sends(hop, way))
            def _():
                line_copy(kv_all, hop, way, 0).wait_send()
                line_copy(z_rows, hop, way, 2).wait_send()

    for hop in range(1, n_pair):
        rank_copy(hop).wait_send()
    for place in range(n_pair):
        slots_copy(place).wait_send()
    for i in range(1, n_ep):
        back_copy(i).wait_send()
    for copies in (hid_copies, att_copies):
        for copy in copies:
            copy.wait_send()


def silu(matrix):
    return matrix / (1.0 + jnp.exp(-matrix))


def on_device(*arguments):
    (mixer_in, mixer_gain, query_weight, key_weight, value_weight, head_lambda) = arguments[:6]
    (head_gain, out_weight, expert_in, expert_gain, routes, route_weights) = arguments[6:12]
    (gate_weight, up_weight, down_weight, shared_gate, shared_up, shared_down) = arguments[12:]
    n_ep, n_tp = lax.axis_size("ep"), lax.axis_size("tp")
    tokens, width = mixer_in.shape
    vdim, qcols, shid = head_gain.shape[0], query_weight.shape[1], shared_gate.shape[1]
    expert_hid = gate_weight.shape[2]
    cap = 2 * tokens * routes.shape[1] // n_ep
    fits = n_tp == 4 and n_ep % 2 == 0 and gate_weight.shape[0] == 1 and cap % 16 == 0
    fits = fits and routes.shape[1] == 2 and head_lambda.shape[0] == 1
    if not fits:
        return on_device_plain(*arguments)
    vmem = pl.BlockSpec(memory_space=pltpu.VMEM)
    hbm = pl.BlockSpec(memory_space=pl.ANY)
    smem = pl.BlockSpec(memory_space=pltpu.SMEM)
    rows = n_tp * tokens
    half_type = jnp.bfloat16
    out_shape = jax.ShapeDtypeStruct((tokens, width), half_type)
    scratch = [
        pltpu.VMEM((width, 2 * qcols + vdim), half_type),
        pltpu.VMEM((width, expert_hid), half_type),
        pltpu.VMEM((width, expert_hid), half_type),
        pltpu.VMEM((expert_hid, width), half_type),
        pltpu.VMEM((width, 2 * shid), half_type),
        pltpu.VMEM((n_tp, tokens, width), half_type),
        pltpu.VMEM((n_tp, tokens, width), half_type),
        pltpu.VMEM((n_tp, vdim, width), half_type),
        pltpu.VMEM((n_tp, shid, width), half_type),
        pltpu.VMEM((n_ep // 2, cap, width), half_type),
        pltpu.VMEM((n_ep, cap, width), half_type),
        pltpu.VMEM((n_ep, cap, width), half_type),
        pltpu.VMEM((n_ep, cap, width), half_type),
        pltpu.VMEM((n_ep, rows, qcols + vdim), half_type),
        pltpu.VMEM((2, rows, qcols), half_type),
        pltpu.VMEM((n_tp, tokens, vdim), half_type),
        pltpu.VMEM((n_tp, tokens, vdim), half_type),
        pltpu.VMEM((n_tp, tokens, shid), half_type),
        pltpu.VMEM((n_tp, tokens, shid), half_type),
        pltpu.VMEM((2, rows, 1), jnp.float32),
        pltpu.VMEM((2, rows, 1), jnp.float32),
        pltpu.VMEM((2, rows, vdim), jnp.float32),
        pltpu.SemaphoreType.DMA((10,)),
        pltpu.SemaphoreType.DMA((12,)),
        pltpu.SemaphoreType.DMA((12,)),
        pltpu.SemaphoreType.DMA((6,)),
        pltpu.SemaphoreType.DMA((6,)),
        pltpu.SemaphoreType.DMA((2, n_ep)),
        pltpu.SemaphoreType.DMA((2, n_ep)),
        pltpu.SemaphoreType.DMA((4, n_ep // 2)),
        pltpu.SemaphoreType.DMA((4, n_ep // 2)),
        pltpu.SemaphoreType.DMA((n_ep // 2,)),
        pltpu.SemaphoreType.DMA((n_ep // 2,)),
        pltpu.VMEM((n_ep // 2, tokens, width), half_type),
        pltpu.VMEM((n_ep // 2, n_ep, tokens), jnp.float32),
        pltpu.SemaphoreType.DMA((n_ep // 2,)),
        pltpu.SemaphoreType.DMA((n_ep // 2,)),
    ]
    return pl.pallas_call(
        functools.partial(fused_kernel, n_ep, cap),
        out_shape=(out_shape, out_shape),
        in_specs=[vmem, vmem, hbm, hbm, hbm, smem, vmem, hbm, vmem, vmem, vmem, vmem]
        + [hbm] * 6,
        out_specs=(vmem, vmem),
        scratch_shapes=scratch,
        compiler_params=pltpu.CompilerParams(collective_id=0, has_side_effects=True),
    )(
        mixer_in,
        mixer_gain[None, :],
        query_weight,
        key_weight,
        value_weight,
        head_lambda,
        head_gain[None, :],
        out_weight,
        expert_in,
        expert_gain[None, :],
        routes.T,
        route_weights.T,
        gate_weight,
        up_weight,
        down_weight,
        shared_gate,
        shared_up,
        shared_down,
    )


def solution(mesh):
    in_specs = (
        P(("ep", "tp"), None),
        P(),
        P(None, "tp"),
        P(None, "tp"),
        P(None, "tp"),
        P("tp"),
        P(),
        P("tp", None),
        P(("ep", "tp"), None),
        P(),
        P(("ep", "tp"), None),
        P(("ep", "tp"), None),
        P("ep", None, None),
        P("ep", None, None),
        P("ep", None, None),
        P(None, "tp"),
        P(None, "tp"),
        P("tp", None),
    )
    out_specs = (P(("ep", "tp"), None), P(("ep", "tp"), None))
    return jax.shard_map(
        on_device, mesh=mesh, in_specs=in_specs, out_specs=out_specs, check_vma=False
    )
```

profile of v0, /device:TPU:0, one launch (start us, length us, event | category | flops | bytes accessed | tf_op | source)
XLA Modules:
  0.0 87.9 jit_solution(13940528286339418250)
XLA Ops:
  1.3 83.0 %shard_map.185 = (bf16[96,2048]{1,0:T(8,128)(2,1)}, bf16[96,2048]{1,0:T(8,128)(2,1)}) custom-call(bf16[96,2048]{1,0:T(8,128)(2,1)} %mixer_in.1, f32[1,2048]{1,0:T(1,128)} %bitcast.5, bf16[2048,128]{1,0:T(8,128)(2,1)} %wq_hbm.1, bf16[2048,128]{1,0:T(8,128)(2,1)} %wk_hbm.1, bf16[2048,128]{1,0:T(8,128)(2,1)} %wv_hbm.1, f32[1]{0:T(128)S(6)} %copy.22.head_lambda, ...), custom_call_target="tpu_custom_call" | custom-call | tf_op jit(solution)/shard_map/pallas_call | solution.py:732
  84.3 1.8 %copy.23 = bf16[96,2048]{1,0:T(8,128)(2,1)} copy(bf16[96,2048]{1,0:T(8,128)(2,1)} %get-tuple-element.4) | data formatting | bytes 786432
  86.1 1.8 %copy.24 = bf16[96,2048]{1,0:T(8,128)(2,1)} copy(bf16[96,2048]{1,0:T(8,128)(2,1)} %get-tuple-element.5) | data formatting | bytes 786432
where the time goes:
time: 89.5 us; the launch traced here: 87.9 us
  Pallas kernels  83 us (93%)
  local copies, waits for them, and re-layouts  3.53 us (4%)
  between operations  1.29 us (1%)
    pallas_call x1, Pallas kernels, on_device(): pl.pallas_call(functools.partial(fused_kernel, n_ep, cap), out_shape=(out...  83 us
    unnamed x2, local copies, waits for them, and re-layouts  3.53 us

commit v1 on v0

v1 whole, which is shorter than its diff:
```python
import functools
import math

import jax
import jax.numpy as jnp
from jax import lax
from jax.experimental import pallas as pl
from jax.experimental.pallas import tpu as pltpu
from jax.sharding import PartitionSpec as P

MESH = pl.DeviceIdType.MESH

EPS = 1e-06
ROUTED_SCALE = 2.5
VMEM_LIMIT = 53 * 1024 * 1024
PIECES = 4
HALVES = 2
SCHEDULE = (
    ("split", 0, 0),
    ("row", None, (-1, 0)),
    ("row", None, (1, 0)),
    ("proj1", None, None),
    ("row", None, (-1, 1)),
    ("wg", None, None),
    ("split", 1, -1),
    ("relay", None, None),
    ("exp", 1, 0),
    ("row", None, (2, 0)),
    ("row", None, (2, 1)),
    ("proj2", None, None),
    ("skv", (1, 0), (1, 0)),
    ("row", None, (1, 1)),
    ("split", 3, 2),
    ("fkv", None, (1, 0)),
    ("fkv", None, (-1, 0)),
    ("split", 2, 1),
    ("ch", (1, 0), None),
    ("far", None, None),
    ("att", 0, 1),
    ("skv", None, (-1, 0)),
    ("ch", (1, 1), None),
    ("exp", 3, 2),
    ("att", 2, -1),
    ("ch", (3, 0), None),
    ("exp", 2, 1),
    ("ch", (3, 1), None),
    ("fkv", None, (2, 0)),
    ("relaye", None, None),
    ("att", 1, 2),
    ("ch", (2, 0), None),
    ("exp", 0, -1),
    ("ch", (3, 2), None),
    ("ch", (3, 3), None),
    ("att", 3, 0),
    ("sendpart", None, None),
    ("ch", None, (2, 0)),
    ("ch", None, (2, 1)),
    ("ch", None, (1, 0)),
    ("ch", (2, 1), (2, 2)),
    ("ch", (2, 2), None),
    ("ch", None, (-1, 0)),
    ("relayw", None, None),
    ("ch", None, (-1, 1)),
    ("ch", None, (2, 3)),
    ("shared", None, None),
    ("ch", None, (1, 1)),
    ("ch", None, (-1, 2)),
    ("ch", (2, 3), None),
    ("ch", (1, 2), None),
    ("ch", (1, 3), None),
    ("ch", None, (1, 2)),
    ("ch", None, (-1, 3)),
    ("merge", None, None),
    ("ch", None, (1, 3)),
    ("gmix", None, None),
    ("gsh", None, None),
    ("final", None, None),
)


def rms_rows(matrix, scales):
    values_in = matrix.astype(jnp.float32)
    inverse = lax.rsqrt(jnp.mean(values_in * values_in, axis=-1, keepdims=True) + EPS)
    return values_in * inverse * scales


def on_device_plain(
    mixer_in,
    mixer_gain,
    query_weight,
    key_weight,
    value_weight,
    head_lambda,
    head_gain,
    out_weight,
    expert_in,
    expert_gain,
    routes,
    route_weights,
    gate_weight,
    up_weight,
    down_weight,
    shared_gate,
    shared_up,
    shared_down,
):
    model_width = mixer_in.shape[1]
    heads_dev = head_lambda.shape[0]
    value_dim = head_gain.shape[0]
    query_cols = query_weight.shape[1]
    half_dim = query_cols // (2 * heads_dev)
    normed_mixer = rms_rows(mixer_in, mixer_gain).astype(jnp.bfloat16)
    normed_expert = rms_rows(expert_in, expert_gain).astype(jnp.bfloat16)
    joined_weight = jnp.concatenate([query_weight, key_weight, value_weight], axis=1)
    projected = jnp.dot(
        lax.all_gather(normed_mixer, "tp", axis=0, tiled=True),
        joined_weight,
        preferred_element_type=jnp.float32,
    ).astype(jnp.bfloat16)
    block_rows = lax.all_gather(normed_expert, "tp", axis=0, tiled=True)
    gate_part = jnp.dot(block_rows, shared_gate, preferred_element_type=jnp.float32)
    up_part = jnp.dot(block_rows, shared_up, preferred_element_type=jnp.float32)
    shared_hidden = (jax.nn.silu(gate_part) * up_part).astype(jnp.bfloat16)
    gathered_rows = projected.shape[0]
    queries = projected[:, :query_cols].reshape(gathered_rows, heads_dev, 2, half_dim)
    key_rows = projected[:, query_cols : 2 * query_cols]
    value_rows = projected[:, 2 * query_cols :]
    scale_factor = half_dim ** (-0.5)

    def attend_block(running, key_block, value_block):
        top_now, total_now, acc_now = running
        span = key_block.shape[0]
        key_heads = key_block.reshape(span, heads_dev, 2, half_dim)
        value_heads = value_block.reshape(span, heads_dev, value_dim)
        scores = (
            jnp.einsum("qhcd,khcd->hcqk", queries, key_heads, preferred_element_type=jnp.float32)
            * scale_factor
        )
        top_next = jnp.maximum(top_now, jnp.max(scores, axis=-1))
        exponent = jnp.exp(scores - top_next[..., None])
        rescale = jnp.exp(top_now - top_next)
        total_next = total_now * rescale + jnp.sum(exponent, axis=-1)
        product = jnp.einsum(
            "hcqk,khe->hcqe",
            exponent.astype(jnp.bfloat16),
            value_heads,
            preferred_element_type=jnp.float32,
        )
        return (top_next, total_next, acc_now * rescale[..., None] + product)

    start_state = (
        jnp.full((heads_dev, 2, gathered_rows), -1e30, jnp.float32),
        jnp.zeros((heads_dev, 2, gathered_rows), jnp.float32),
        jnp.zeros((heads_dev, 2, gathered_rows, value_dim), jnp.float32),
    )
    key_piece = lax.all_gather(key_rows, "ep", axis=0, tiled=True)
    value_piece = lax.all_gather(value_rows, "ep", axis=0, tiled=True)
    span = key_piece.shape[0]
    block_len = math.gcd(span, 4 * gathered_rows)
    steps_count = span // block_len
    key_blocks = key_piece.reshape(steps_count, block_len, key_piece.shape[1])
    value_blocks = value_piece.reshape(steps_count, block_len, value_piece.shape[1])

    def step_once(state, blocks):
        return (attend_block(state, blocks[0], blocks[1]), None)

    result, unused = lax.scan(step_once, start_state, (key_blocks, value_blocks))
    top_all, total_all, acc_all = result
    read_out = acc_all / total_all[..., None]
    lambda_col = head_lambda[:, None, None]
    difference = read_out[:, 0] - lambda_col * read_out[:, 1]
    head_out = rms_rows(difference, head_gain) * (1.0 - lambda_col)
    attended = (
        jnp.transpose(head_out, (1, 0, 2))
        .reshape(gathered_rows, heads_dev * value_dim)
        .astype(jnp.bfloat16)
    )
    token_count = routes.shape[0]
    top_count = routes.shape[1]
    ep_count = lax.axis_size("ep")
    local_experts = gate_weight.shape[0]
    expert_count = ep_count * local_experts
    capacity = 2 * token_count * top_count // expert_count
    flat_routes = routes.reshape(-1)
    onehot = (flat_routes[:, None] == jnp.arange(expert_count, dtype=jnp.int32)[None, :]).astype(
        jnp.int32
    )
    earlier = jnp.cumsum(onehot, axis=0) - onehot
    slot_rank = jnp.sum(earlier * onehot, axis=1)
    slot_index = flat_routes * capacity + slot_rank
    owners = jnp.arange(token_count * top_count, dtype=jnp.int32) // top_count
    source = jnp.full((expert_count * capacity,), token_count, jnp.int32).at[slot_index].set(owners)
    padded = jnp.concatenate([normed_expert, jnp.zeros((1, model_width), jnp.bfloat16)], axis=0)
    outgoing = padded[source].reshape(ep_count, local_experts, capacity, model_width)
    arrived = lax.all_to_all(outgoing, "ep", split_axis=0, concat_axis=0, tiled=True)
    gate_part = jnp.einsum(
        "sxcd,xdf->sxcf", arrived, gate_weight, preferred_element_type=jnp.float32
    )
    up_part = jnp.einsum("sxcd,xdf->sxcf", arrived, up_weight, preferred_element_type=jnp.float32)
    hidden = (jax.nn.silu(gate_part) * up_part).astype(jnp.bfloat16)
    result = jnp.einsum(
        "sxcf,xfd->sxcd", hidden, down_weight, preferred_element_type=jnp.float32
    ).astype(jnp.bfloat16)
    returned = lax.all_to_all(result, "ep", split_axis=0, concat_axis=0, tiled=True)
    picked = returned.reshape(expert_count * capacity, model_width)[slot_index]
    picked = picked.reshape(token_count, top_count, model_width)
    shares = ROUTED_SCALE * route_weights / jnp.sum(route_weights, axis=1, keepdims=True)
    routed = jnp.sum(shares[:, :, None] * picked.astype(jnp.float32), axis=1)
    rows_here = attended
    mixer_sum = lax.psum_scatter(
        jnp.dot(rows_here, out_weight, preferred_element_type=jnp.float32).astype(jnp.bfloat16),
        "tp",
        scatter_dimension=0,
        tiled=True,
    )
    rows_here = shared_hidden
    shared_sum = lax.psum_scatter(
        jnp.dot(rows_here, shared_down, preferred_element_type=jnp.float32).astype(jnp.bfloat16),
        "tp",
        scatter_dimension=0,
        tiled=True,
    ).astype(jnp.float32)
    expert_out = (routed + shared_sum).astype(jnp.bfloat16)
    return (mixer_sum, expert_out)


def fused_kernel(
    n_ep,
    cap,
    mixer_in_hbm,
    mixer_gain_hbm,
    wq_hbm,
    wk_hbm,
    wv_hbm,
    head_lambda,
    head_gain_hbm,
    wo_hbm,
    expert_in_hbm,
    expert_gain_hbm,
    routes_hbm,
    weights_hbm,
    gate_hbm,
    up_hbm,
    down_hbm,
    sgate_hbm,
    sup_hbm,
    sdown_hbm,
    mixed_out,
    expert_out,
    mixer_in,
    mixer_gain,
    head_gain,
    expert_in,
    expert_gain,
    routes_t,
    weights_t,
    w_qkv,
    w_gate,
    w_up,
    w_down,
    w_sh,
    g_mix,
    g_exp,
    g_wo,
    g_wsd,
    outgoing,
    arrived,
    pair,
    back,
    combine,
    chain_out,
    chain_in,
    part_ref,
    temp_ref,
    kv_all,
    q_raw,
    q_far,
    q_two,
    read_out,
    read_in,
    lse_out,
    lse_in,
    att_mine,
    att_all,
    hid_mine,
    hid_all,
    top_ref,
    total_ref,
    acc_ref,
    z_rows,
    ranks,
    load_sem,
    tp_send,
    tp_recv,
    small_send,
    small_recv,
    rank_send,
    rank_recv,
    row_send,
    row_recv,
    kv_send,
    kv_recv,
    slots_send,
    slots_recv,
    back_send,
    back_recv,
    chain_send,
    chain_recv,
    twin_send,
    twin_recv,
):
    me = lax.axis_index("ep")
    tp = lax.axis_index("tp")
    near = tp + 1 - 2 * lax.rem(tp, 2)
    far = lax.rem(tp + 2, 4)
    cross = lax.rem(near + 2, 4)
    n_pair = n_ep // 2
    tokens, width = mixer_in.shape
    vdim = head_gain.shape[1]
    qcols = wq_hbm.shape[1]
    shid = sgate_hbm.shape[1]
    half = qcols // 2
    rows = 4 * tokens
    piece_cols = width // PIECES
    half_rows = tokens // HALVES

    line, low = me // 2, lax.rem(me, 2)
    twin = 2 * line + 1 - low
    last = n_pair - 1
    end_int = line // last + (last - line) // last
    is_end = end_int == 1
    is_inner = end_int == 0
    inward_way = line // (n_pair // 2)
    inward = 1 - 2 * inward_way

    small_pairs = (
        (mixer_in_hbm, mixer_in),
        (mixer_gain_hbm, mixer_gain),
        (expert_in_hbm, expert_in),
        (expert_gain_hbm, expert_gain),
        (routes_hbm, routes_t),
        (weights_hbm, weights_t),
        (head_gain_hbm, head_gain),
    )
    firsts = []
    for number, (origin, target) in enumerate(small_pairs):
        load = pltpu.make_async_copy(origin, target, load_sem.at[10 + number])
        load.start()
        firsts.append(load)

    def column_peer(hop):
        return 2 * lax.rem(line + hop, n_pair) + low

    barrier = pltpu.get_barrier_semaphore()
    for other in (near, far, cross):
        pl.semaphore_signal(barrier, inc=1, device_id=(me, other), device_id_type=MESH)
    pl.semaphore_signal(barrier, inc=1, device_id=(twin, tp), device_id_type=MESH)
    for hop in range(1, n_pair):
        pl.semaphore_signal(
            barrier, inc=1, device_id=(column_peer(hop), tp), device_id_type=MESH
        )

    pairs = (
        (wq_hbm, w_qkv.at[:, 0:qcols]),
        (wk_hbm, w_qkv.at[:, qcols : 2 * qcols]),
        (wv_hbm, w_qkv.at[:, 2 * qcols : 2 * qcols + vdim]),
        (sdown_hbm, g_wsd.at[tp]),
        (wo_hbm, g_wo.at[tp]),
        (gate_hbm.at[0], w_gate),
        (up_hbm.at[0], w_up),
        (down_hbm.at[0], w_down),
        (sgate_hbm, w_sh.at[:, 0:shid]),
        (sup_hbm, w_sh.at[:, shid : 2 * shid]),
    )
    loads = []
    for number, (origin, target) in enumerate(pairs):
        load = pltpu.make_async_copy(origin, target, load_sem.at[number])
        load.start()
        loads.append(load)

    def remote(origin, target, send_sem, recv_sem, device):
        return pltpu.make_async_remote_copy(
            src_ref=origin,
            dst_ref=target,
            send_sem=send_sem,
            recv_sem=recv_sem,
            device_id=device,
            device_id_type=MESH,
        )

    def tp_copy(buf, slot, other, number):
        place = buf.at[slot]
        return remote(place, place, tp_send.at[number], tp_recv.at[number], (me, other))

    def gather_start(buf, number):
        to_far = tp_copy(buf, tp, far, 3 * number)
        to_near = tp_copy(buf, tp, near, 3 * number + 1)
        to_far.start()
        to_near.start()
        return to_far, to_near

    def relay_start(buf, number, copies):
        copies[0].wait_recv()
        relay = tp_copy(buf, far, near, 3 * number + 2)
        relay.start()
        return relay

    def beside(way):
        return (2 * lax.rem(line + 1 - 2 * way + n_pair, n_pair) + low, tp)

    def row_copy(place, number, way):
        block = z_rows.at[place, pl.ds(number * half_rows, half_rows), :]
        return remote(
            block, block, row_send.at[way, place, number], row_recv.at[place, number], beside(way)
        )

    def kv_copy(place, way):
        block = kv_all.at[place]
        return remote(block, block, kv_send.at[way, place], kv_recv.at[place], beside(way))

    def rank_copy(hop):
        block = ranks.at[line]
        return remote(
            block, block, rank_send.at[hop], rank_recv.at[hop], (column_peer(hop), tp)
        )

    def slots_copy(place):
        return remote(
            outgoing.at[place],
            arrived.at[place, 1],
            slots_send.at[place],
            slots_recv.at[place],
            (twin, tp),
        )

    def back_copy(place, piece):
        return remote(
            back.at[place, piece],
            pair.at[place, piece, 1],
            back_send.at[place, piece],
            back_recv.at[place, piece],
            (twin, tp),
        )

    def chain_copy(place, piece, way):
        return remote(
            chain_out.at[place, piece],
            chain_in.at[way, place, piece],
            chain_send.at[place, piece],
            chain_recv.at[way, place, piece],
            beside(way),
        )

    def twin_copy(origin, target, number):
        return remote(origin, target, twin_send.at[number], twin_recv.at[number], (twin, tp))

    firsts[0].wait()
    firsts[1].wait()
    g_mix[tp] = rms_rows(mixer_in[...], mixer_gain[...]).astype(jnp.bfloat16)
    pl.semaphore_wait(barrier, n_pair + 3)
    mix_copies = gather_start(g_mix, 0)
    firsts[2].wait()
    firsts[3].wait()
    normed = rms_rows(expert_in[...], expert_gain[...]).astype(jnp.bfloat16)
    g_exp[tp] = normed
    z_rows[line] = normed
    for number in range(HALVES):
        row_copy(line, number, inward_way).start()

        @pl.when(is_inner)
        def _():
            row_copy(line, number, 1 - inward_way).start()

    exp_copies = gather_start(g_exp, 1)

    for number in range(4, 7):
        firsts[number].wait()
    expert_row = lax.broadcasted_iota(jnp.int32, (n_ep, tokens), 0)
    first, second = routes_t[0:1, :] == expert_row, routes_t[1:2, :] == expert_row
    named = jnp.logical_or(first, second)
    before = (
        lax.broadcasted_iota(jnp.int32, (tokens, tokens), 0)
        < lax.broadcasted_iota(jnp.int32, (tokens, tokens), 1)
    )
    rank = jnp.dot(
        jnp.where(named, 1.0, 0.0).astype(jnp.bfloat16),
        jnp.where(before, 1.0, 0.0).astype(jnp.bfloat16),
        preferred_element_type=jnp.float32,
    )
    scale = ROUTED_SCALE / (weights_t[0:1, :] + weights_t[1:2, :])
    share = jnp.where(first, weights_t[0:1, :] * scale, 0.0)
    share = share + jnp.where(second, weights_t[1:2, :] * scale, 0.0)
    ranks[line, 0:n_ep, :] = jnp.where(named, rank, -1.0)
    ranks[line, n_ep : 2 * n_ep, :] = share
    for hop in range(1, n_pair):
        rank_copy(hop).start()
    slot = lax.broadcasted_iota(jnp.int32, (cap, tokens), 0).astype(jnp.float32)

    top_ref[...] = jnp.full_like(top_ref, -1e30)
    total_ref[...] = jnp.zeros_like(total_ref)
    acc_ref[...] = jnp.zeros_like(acc_ref)
    held = {}

    def project(chip):
        block = g_mix[pl.ds(2 * chip, 2)].reshape(2 * tokens, width)
        out = jnp.dot(block, w_qkv[...], preferred_element_type=jnp.float32).astype(jnp.bfloat16)
        place = pl.ds(pl.multiple_of(2 * chip * tokens, 2 * tokens), 2 * tokens)
        kv_all[line, place, :] = out[:, qcols:]
        queries = (out[:, :qcols].astype(jnp.float32) * (half ** (-0.5))).astype(jnp.bfloat16)
        q_raw[place, :] = queries
        spread_halves(queries, place)

    def spread_halves(queries, place):
        wide = queries.astype(jnp.float32)
        lane = lax.broadcasted_iota(jnp.int32, wide.shape, 1)
        q_two[0, place, :] = jnp.where(lane < half, wide, 0.0).astype(jnp.bfloat16)
        q_two[1, place, :] = jnp.where(lane < half, 0.0, wide).astype(jnp.bfloat16)

    def task_split(place, at_end, at_inner):
        def wait_rank():
            rank_copy(lax.rem(line - place + n_pair, n_pair)).wait_recv()

        if at_end != 0:

            @pl.when(is_end)
            def _():
                for number in range(HALVES):
                    row_copy(place, number, 0).wait_recv()
                wait_rank()

        if at_inner != 0:

            @pl.when(is_inner)
            def _():
                wait_rank()

        wanted = [ranks[place, pl.ds(e, 1), :] == slot for e in (twin, me)]
        picks = jnp.concatenate([jnp.where(c, 1.0, 0.0) for c in wanted], axis=0)
        moved = jnp.dot(
            picks.astype(jnp.bfloat16), z_rows[place], preferred_element_type=jnp.float32
        ).astype(jnp.bfloat16)
        outgoing[place] = moved[:cap]
        slots_copy(place).start()
        arrived[place, 0] = moved[cap:]
        share_of = [ranks[place, pl.ds(n_ep + e, 1), :] for e in (twin, me)]
        weights = [jnp.where(c, g, 0.0) for c, g in zip(wanted, share_of)]
        weights = jnp.concatenate([weights[1], weights[0]], axis=0)
        high = weights.astype(jnp.bfloat16)
        combine[place, 0] = high
        combine[place, 1] = (weights - high.astype(jnp.float32)).astype(jnp.bfloat16)

    def task_exp(place, at_end, at_inner):
        if "experts" not in held:
            held["experts"] = True
            for number in range(5, 8):
                loads[number].wait()
        slots_copy(place).wait_recv()
        taken = arrived[place].reshape(2 * cap, width)
        gate_part = jnp.dot(taken, w_gate[...], preferred_element_type=jnp.float32)
        up_part = jnp.dot(taken, w_up[...], preferred_element_type=jnp.float32)
        hidden = (silu(gate_part) * up_part).astype(jnp.bfloat16)
        for piece in range(PIECES):
            answer = jnp.dot(
                hidden,
                w_down[:, piece * piece_cols : (piece + 1) * piece_cols],
                preferred_element_type=jnp.float32,
            ).astype(jnp.bfloat16)
            back[place, piece] = answer[cap:]
            back_copy(place, piece).start()
            pair[place, piece, 0] = answer[:cap]

    def combined(place, piece):
        back_copy(place, piece).wait_recv()
        answers = pair[place, piece].reshape(2 * cap, piece_cols)
        total = None
        for term in range(2):
            product = lax.dot_general(
                combine[place, term],
                answers,
                (((0,), (0,)), ((), ())),
                preferred_element_type=jnp.float32,
            )
            total = product if total is None else total + product
        return total

    def task_ch(place, piece, way, joins):
        value = combined(place, piece)
        if joins is None:
            chain_out[place, piece] = value.astype(jnp.bfloat16)
        elif joins is True:
            chain_copy(place, piece, way).wait_recv()
            chain_out[place, piece] = (
                value + chain_in[way, place, piece].astype(jnp.float32)
            ).astype(jnp.bfloat16)
        else:
            temp_ref[...] = value

            @pl.when(joins)
            def _():
                chain_copy(place, piece, way).wait_recv()
                temp_ref[...] = temp_ref[...] + chain_in[way, place, piece].astype(jnp.float32)

            chain_out[place, piece] = temp_ref[...].astype(jnp.bfloat16)

        chain_copy(place, piece, way).start()

    q_chunk = 2 * rows // 3

    def task_att(place, at_end, at_inner):
        if at_end != 0:

            @pl.when(is_end)
            def _():
                kv_copy(place, 0).wait_recv()

        keys = kv_all[place, :, 0:qcols]
        values_t = jnp.transpose(kv_all[place, :, qcols : qcols + vdim])
        ids = [(c, slice(r * q_chunk, (r + 1) * q_chunk)) for r in range(3) for c in range(2)]
        for c, part in ids:
            scores = lax.dot_general(
                keys,
                q_two[c, part, :],
                (((1,), (1,)), ((), ())),
                preferred_element_type=jnp.float32,
            )
            top_now = top_ref[c : c + 1, part]
            top_next = jnp.maximum(top_now, jnp.max(scores, axis=0, keepdims=True))
            exponent = jnp.exp(scores - top_next)
            rescale = jnp.exp(top_now - top_next)
            top_ref[c : c + 1, part] = top_next
            total_ref[c : c + 1, part] = total_ref[c : c + 1, part] * rescale + jnp.sum(
                exponent, axis=0, keepdims=True
            )
            acc_ref[c, :, part] = acc_ref[c, :, part] * rescale + jnp.dot(
                values_t, exponent.astype(jnp.bfloat16), preferred_element_type=jnp.float32
            )

    def spread(mine, everyone, base):
        copies = []
        for k, other in enumerate((near, far, cross)):
            copy = remote(
                mine.at[other],
                everyone.at[tp],
                small_send.at[base + k],
                small_recv.at[base + k],
                (me, other),
            )
            copy.start()
            copies.append(copy)
        everyone[tp] = mine[tp]
        return copies

    def grouped(rows_all, weight_all):
        total = None
        for g in range(4):
            piece = (
                jnp.dot(rows_all[g], weight_all[g], preferred_element_type=jnp.float32)
                .astype(jnp.bfloat16)
                .astype(jnp.float32)
            )
            total = piece if total is None else total + piece
        return total

    q_copy = twin_copy(q_raw, q_far, 0)
    read_copy = twin_copy(read_out, read_in, 1)
    lse_copy = twin_copy(lse_out, lse_in, 2)

    def task_wg():
        loads[3].wait()
        held["wsd"] = gather_start(g_wsd, 2)
        loads[4].wait()
        held["wo"] = gather_start(g_wo, 3)

    def task_proj1():
        for number in range(3):
            loads[number].wait()
        mix_copies[1].wait_recv()
        project(tp // 2)

    def task_relay():
        held["mix_relay"] = relay_start(g_mix, 0, mix_copies)

    def task_proj2():
        held["mix_relay"].wait_recv()
        project(far // 2)
        q_copy.start()

    def task_far():
        q_copy.wait_recv()
        spread_halves(q_far[...], slice(rows, 2 * rows))

    def task_relaye():
        held["exp_relay"] = relay_start(g_exp, 1, exp_copies)

    def task_shared():
        exp_copies[1].wait_recv()
        loads[8].wait()
        loads[9].wait()
        held["exp_relay"].wait_recv()
        both = jnp.dot(
            g_exp[...].reshape(rows, width), w_sh[...], preferred_element_type=jnp.float32
        )
        hid_mine[...] = (
            (silu(both[:, :shid]) * both[:, shid:]).astype(jnp.bfloat16).reshape(4, tokens, shid)
        )
        held["hid"] = spread(hid_mine, hid_all, 0)

    def task_relayw():
        held["wsd_relay"] = relay_start(g_wsd, 2, held["wsd"])
        held["wo_relay"] = relay_start(g_wo, 3, held["wo"])

    def task_gsh():
        held["wsd"][1].wait_recv()
        held["wsd_relay"].wait_recv()
        for copy in held["hid"]:
            copy.wait_recv()
        part_ref[...] = grouped(hid_all, g_wsd)

    def task_sendpart():
        place = slice(rows, 2 * rows)
        for c in range(2):
            read_out[c] = (acc_ref[c, :, place] / total_ref[c : c + 1, place]).astype(
                jnp.bfloat16
            )
            lse_out[c : c + 1, :] = top_ref[c : c + 1, place] + jnp.log(
                total_ref[c : c + 1, place]
            )
        read_copy.start()
        lse_copy.start()

    def task_merge():
        lam = head_lambda[0]
        lse_copy.wait_recv()
        read_copy.wait_recv()
        reads = []
        for c in range(2):
            total = total_ref[c : c + 1, 0:rows]
            lse_mine = top_ref[c : c + 1, 0:rows] + jnp.log(total)
            lse_far = lse_in[c : c + 1, :]
            best = jnp.maximum(lse_mine, lse_far)
            mine = jnp.exp(lse_mine - best)
            theirs = jnp.exp(lse_far - best)
            both = mine + theirs
            reads.append(
                acc_ref[c, :, 0:rows] * (mine / (both * total))
                + read_in[c].astype(jnp.float32) * (theirs / both)
            )
        difference = reads[0] - lam * reads[1]
        inverse = lax.rsqrt(jnp.mean(difference * difference, axis=0, keepdims=True) + EPS)
        head_out = jnp.transpose(difference * inverse) * head_gain[...] * (1.0 - lam)
        att_mine[...] = head_out.astype(jnp.bfloat16).reshape(4, tokens, vdim)
        held["att"] = spread(att_mine, att_all, 3)

    def task_gmix():
        held["wo"][1].wait_recv()
        held["wo_relay"].wait_recv()
        for copy in held["att"]:
            copy.wait_recv()
        mixed_out[...] = grouped(att_all, g_wo).astype(jnp.bfloat16)

    def task_final():
        for piece in range(PIECES):
            cols = slice(piece * piece_cols, (piece + 1) * piece_cols)
            chain_copy(line, piece, 1 - inward_way).wait_recv()
            value = (
                part_ref[:, cols]
                + combined(line, piece)
                + chain_in[1 - inward_way, line, piece].astype(jnp.float32)
            )
            part_ref[:, cols] = value

            @pl.when(is_inner)
            def _():
                chain_copy(line, piece, inward_way).wait_recv()
                part_ref[:, cols] = part_ref[:, cols] + chain_in[
                    inward_way, line, piece
                ].astype(jnp.float32)

            expert_out[:, cols] = part_ref[:, cols].astype(jnp.bfloat16)

    plain = {
        "wg": task_wg,
        "proj1": task_proj1,
        "relay": task_relay,
        "proj2": task_proj2,
        "far": task_far,
        "relaye": task_relaye,
        "shared": task_shared,
        "relayw": task_relayw,
        "gsh": task_gsh,
        "sendpart": task_sendpart,
        "merge": task_merge,
        "gmix": task_gmix,
        "final": task_final,
    }
    placed = {"split": task_split, "exp": task_exp, "att": task_att}

    def toward(hop):
        return inward_way if hop > 0 else 1 - inward_way

    def one_class(kind, hop, number):
        place = line + inward * hop
        if kind == "row":
            row_copy(place, number, 0).wait_recv()
            row_copy(place, number, toward(-hop)).start()
        elif kind == "skv":
            kv_copy(line, toward(hop)).start()
        else:
            kv_copy(place, 0).wait_recv()
            kv_copy(place, toward(-hop)).start()

    for kind, at_end, at_inner in SCHEDULE:
        if kind in plain:
            plain[kind]()
        elif kind in placed:
            hop = at_inner + (at_end - at_inner) * end_int
            placed[kind](line + inward * hop, at_end, at_inner)
        elif kind == "ch":
            if at_end is not None and at_inner is not None and at_inner[0] > 0:
                hop = at_inner[0] + (at_end[0] - at_inner[0]) * end_int
                piece = at_inner[1] + (at_end[1] - at_inner[1]) * end_int
                task_ch(line + inward * hop, piece, inward_way, is_inner)
            else:
                if at_end is not None:

                    @pl.when(is_end)
                    def _():
                        task_ch(line + inward * at_end[0], at_end[1], inward_way, None)

                if at_inner is not None:

                    @pl.when(is_inner)
                    def _():
                        task_ch(
                            line + inward * at_inner[0],
                            at_inner[1],
                            toward(at_inner[0]),
                            True,
                        )

        elif at_end is not None and at_end == at_inner:
            one_class(kind, *at_end)
        else:
            for chosen, spot in ((is_end, at_end), (is_inner, at_inner)):
                if spot is not None:

                    @pl.when(chosen)
                    def _():
                        one_class(kind, *spot)

    for copies in (mix_copies, exp_copies, held["wsd"], held["wo"]):
        for copy in copies:
            copy.wait_send()
    for name in ("mix_relay", "exp_relay", "wsd_relay", "wo_relay"):
        held[name].wait_send()
    for copies in (held["hid"], held["att"]):
        for copy in copies:
            copy.wait_send()
    for copy in (q_copy, read_copy, lse_copy):
        copy.wait_send()
    for hop in range(1, n_pair):
        rank_copy(hop).wait_send()
    for place in range(n_pair):
        slots_copy(place).wait_send()
        for piece in range(PIECES):
            back_copy(place, piece).wait_send()
    for number in range(HALVES):
        row_copy(line, number, inward_way).wait_send()
    kv_copy(line, inward_way).wait_send()
    for piece in range(PIECES):
        chain_copy(line + inward, piece, inward_way).wait_send()
        chain_copy(line + 2 * inward, piece, inward_way).wait_send()

    @pl.when(is_end)
    def _():
        for piece in range(PIECES):
            chain_copy(line + 3 * inward, piece, inward_way).wait_send()

    @pl.when(is_inner)
    def _():
        for piece in range(PIECES):
            chain_copy(line - inward, piece, 1 - inward_way).wait_send()
        kv_copy(line, 1 - inward_way).wait_send()
        for hop in (1, 2, -1):
            place = line + inward * hop
            kv_copy(place, toward(-hop)).wait_send()
            for number in range(HALVES):
                row_copy(place, number, toward(-hop)).wait_send()
        for number in range(HALVES):
            row_copy(line, number, 1 - inward_way).wait_send()


def silu(matrix):
    return matrix / (1.0 + jnp.exp(-matrix))


def on_device(*arguments):
    (mixer_in, mixer_gain, query_weight, key_weight, value_weight, head_lambda) = arguments[:6]
    (head_gain, out_weight, expert_in, expert_gain, routes, route_weights) = arguments[6:12]
    (gate_weight, up_weight, down_weight, shared_gate, shared_up, shared_down) = arguments[12:]
    n_ep, n_tp = lax.axis_size("ep"), lax.axis_size("tp")
    tokens, width = mixer_in.shape
    vdim, qcols, shid = head_gain.shape[0], query_weight.shape[1], shared_gate.shape[1]
    expert_hid = gate_weight.shape[2]
    cap = 2 * tokens * routes.shape[1] // n_ep
    fits = n_tp == 4 and n_ep % 2 == 0 and gate_weight.shape[0] == 1 and cap % 16 == 0
    fits = fits and routes.shape[1] == 2 and head_lambda.shape[0] == 1
    if not fits:
        return on_device_plain(*arguments)
    if n_ep != 8 or tokens % (16 * HALVES) or width % (128 * PIECES):
        return on_device_plain(*arguments)
    vmem = pl.BlockSpec(memory_space=pltpu.VMEM)
    hbm = pl.BlockSpec(memory_space=pltpu.HBM)
    smem = pl.BlockSpec(memory_space=pltpu.SMEM)
    rows, n_pair = n_tp * tokens, n_ep // 2
    half_type = jnp.bfloat16
    piece_cols = width // PIECES
    out_shape = jax.ShapeDtypeStruct((tokens, width), half_type)
    dma = pltpu.SemaphoreType.DMA
    scratch = [
        pltpu.VMEM((tokens, width), half_type),
        pltpu.VMEM((1, width), jnp.float32),
        pltpu.VMEM((1, vdim), jnp.float32),
        pltpu.VMEM((tokens, width), half_type),
        pltpu.VMEM((1, width), jnp.float32),
        pltpu.VMEM((2, tokens), jnp.int32),
        pltpu.VMEM((2, tokens), jnp.float32),
        pltpu.VMEM((width, 2 * qcols + vdim), half_type),
        pltpu.VMEM((width, expert_hid), half_type),
        pltpu.VMEM((width, expert_hid), half_type),
        pltpu.VMEM((expert_hid, width), half_type),
        pltpu.VMEM((width, 2 * shid), half_type),
        pltpu.VMEM((n_tp, tokens, width), half_type),
        pltpu.VMEM((n_tp, tokens, width), half_type),
        pltpu.VMEM((n_tp, vdim, width), half_type),
        pltpu.VMEM((n_tp, shid, width), half_type),
        pltpu.VMEM((n_pair, cap, width), half_type),
        pltpu.VMEM((n_pair, 2, cap, width), half_type),
        pltpu.VMEM((n_pair, PIECES, 2, cap, piece_cols), half_type),
        pltpu.VMEM((n_pair, PIECES, cap, piece_cols), half_type),
        pltpu.VMEM((n_pair, 2, 2 * cap, tokens), half_type),
        pltpu.VMEM((n_pair, PIECES, tokens, piece_cols), half_type),
        pltpu.VMEM((2, n_pair, PIECES, tokens, piece_cols), half_type),
        pltpu.VMEM((tokens, width), jnp.float32),
        pltpu.VMEM((tokens, piece_cols), jnp.float32),
        pltpu.VMEM((n_pair, rows, qcols + vdim), half_type),
        pltpu.VMEM((rows, qcols), half_type),
        pltpu.VMEM((rows, qcols), half_type),
        pltpu.VMEM((2, 2 * rows, qcols), half_type),
        pltpu.VMEM((2, vdim, rows), half_type),
        pltpu.VMEM((2, vdim, rows), half_type),
        pltpu.VMEM((2, rows), jnp.float32),
        pltpu.VMEM((2, rows), jnp.float32),
        pltpu.VMEM((n_tp, tokens, vdim), half_type),
        pltpu.VMEM((n_tp, tokens, vdim), half_type),
        pltpu.VMEM((n_tp, tokens, shid), half_type),
        pltpu.VMEM((n_tp, tokens, shid), half_type),
        pltpu.VMEM((2, 2 * rows), jnp.float32),
        pltpu.VMEM((2, 2 * rows), jnp.float32),
        pltpu.VMEM((2, vdim, 2 * rows), jnp.float32),
        pltpu.VMEM((n_pair, tokens, width), half_type),
        pltpu.VMEM((n_pair, 2 * n_ep, tokens), jnp.float32),
        dma((17,)),
        dma((12,)),
        dma((12,)),
        dma((6,)),
        dma((6,)),
        dma((n_pair,)),
        dma((n_pair,)),
        dma((2, n_pair, HALVES)),
        dma((n_pair, HALVES)),
        dma((2, n_pair)),
        dma((n_pair,)),
        dma((n_pair,)),
        dma((n_pair,)),
        dma((n_pair, PIECES)),
        dma((n_pair, PIECES)),
        dma((n_pair, PIECES)),
        dma((2, n_pair, PIECES)),
        dma((3,)),
        dma((3,)),
    ]
    return pl.pallas_call(
        functools.partial(fused_kernel, n_ep, cap),
        out_shape=(out_shape, out_shape),
        in_specs=[hbm] * 5 + [smem] + [hbm] * 12,
        out_specs=(vmem, vmem),
        scratch_shapes=scratch,
        compiler_params=pltpu.CompilerParams(
            collective_id=0, has_side_effects=True, vmem_limit_bytes=VMEM_LIMIT
        ),
    )(
        mixer_in,
        mixer_gain[None, :],
        query_weight,
        key_weight,
        value_weight,
        head_lambda,
        head_gain[None, :],
        out_weight,
        expert_in,
        expert_gain[None, :],
        routes.T,
        route_weights.T,
        gate_weight,
        up_weight,
        down_weight,
        shared_gate,
        shared_up,
        shared_down,
    )


def solution(mesh):
    in_specs = (
        P(("ep", "tp"), None),
        P(),
        P(None, "tp"),
        P(None, "tp"),
        P(None, "tp"),
        P("tp"),
        P(),
        P("tp", None),
        P(("ep", "tp"), None),
        P(),
        P(("ep", "tp"), None),
        P(("ep", "tp"), None),
        P("ep", None, None),
        P("ep", None, None),
        P("ep", None, None),
        P(None, "tp"),
        P(None, "tp"),
        P("tp", None),
    )
    out_specs = (P(("ep", "tp"), None), P(("ep", "tp"), None))
    return jax.shard_map(
        on_device, mesh=mesh, in_specs=in_specs, out_specs=out_specs, check_vma=False
    )
```

time: 89.5 us -> 73.4 us (0.82); the launches traced: 87.9 us -> 72.7 us
  Pallas kernels: 83 us -> 66.5 us
  local copies, waits for them, and re-layouts: 3.53 us -> 4.89 us
    pallas_call x1, Pallas kernels: 83 us -> 66.5 us  [on_device(): pl.pallas_call(functools.partial(fused_kernel, n_ep, cap), out_shape=(out...]
    unnamed x2 -> x12, local copies, waits for them, and re-layouts: 3.53 us -> 4.89 us
where the time goes in v1:
time: 73.4 us; the launch traced here: 72.7 us
  Pallas kernels  66.5 us (91%)
  local copies, waits for them, and re-layouts  4.89 us (7%)
  between operations  1.3 us (2%)
    pallas_call x1, Pallas kernels, on_device(): pl.pallas_call(functools.partial(fused_kernel, n_ep, cap), out_shape=(out...  66.5 us
    unnamed x12, local copies, waits for them, and re-layouts  4.89 us

profile of v1, /device:TPU:0, one launch (start us, length us, event | category | flops | bytes accessed | tf_op | source)
XLA Modules:
  0.0 72.7 jit_solution(11512324814989970675)
XLA Ops:
  1.3 0.0 copy-start
  1.3 0.7 copy-done
  2.0 0.0 copy-start.1
  2.0 0.7 copy-done.1
  2.7 0.0 copy-start.2
  2.7 0.7 copy-done.2
  3.4 0.0 copy-start.3
  3.4 0.7 copy-done.3
  4.0 0.0 copy-start.4
  4.0 0.7 copy-done.4
  4.7 66.5 %shard_map.185 = (bf16[96,2048]{1,0:T(8,128)(2,1)S(1)}, bf16[96,2048]{1,0:T(8,128)(2,1)S(1)}) custom-call(bf16[96,2048]{1,0:T(8,128)(2,1)} %mixer_in_hbm.1, f32[1,2048]{1,0:T(1,128)S(1)} %bitcast.5, bf16[2048,128]{1,0:T(8,128)(2,1)} %wq_hbm.1, bf16[2048,128]{1,0:T(8,128)(2,1)} %wk_hbm.1, bf16[2048,128]{1,0:T(8,128)(2,1)} %wv_hbm.1, f32[1]{0:T(128)S(6)} %copy.22.head_lambda, ...), custom_call_target="tpu_custom_call" | custom-call | tf_op jit(solution)/shard_map/pallas_call | solution.py:983
  71.2 0.7 %copy.23 = bf16[96,2048]{1,0:T(8,128)(2,1)} copy(bf16[96,2048]{1,0:T(8,128)(2,1)S(1)} %get-tuple-element.4) | data formatting | bytes 786432
  72.0 0.7 %copy.24 = bf16[96,2048]{1,0:T(8,128)(2,1)} copy(bf16[96,2048]{1,0:T(8,128)(2,1)S(1)} %get-tuple-element.5) | data formatting | bytes 786432
Async XLA Ops:
  1.3 0.7 copy-start
  2.0 0.7 copy-start.1
  2.7 0.7 copy-start.2
  3.4 0.7 copy-start.3
  4.0 0.7 copy-start.4
